TPU v7x, 512 devices: a whole 4x4x16 slice. The times are simulated.
512 devices in a mesh: sp: 64 (over z, y), tp: 8 (over x, core).
Axes of the slice: x: 4, y: 4, z: 16, core: 2. Of those that a mesh axis runs over, the one named last changes fastest.
Arguments:
- target: bfloat16 [8192, 2048], P('sp'), may hold values from -0.375 to 0.375
- source: bfloat16 [16384, 2048], P(('sp', 'tp')), may hold values from -0.375 to 0.375
- target_gain: float32 [2048], replicated, may hold values from 0.3 to 12
- source_gain: float32 [2048], replicated, may hold values from 0.3 to 12
- w_query: bfloat16 [2048, 1024], P(None, 'tp'), may hold values from -0.125 to 0.125
- w_key: bfloat16 [2048, 256], replicated, may hold values from -0.125 to 0.125
- w_value: bfloat16 [2048, 256], replicated, may hold values from -0.125 to 0.125
- attended: bfloat16 [8192, 1024], P('sp', 'tp'), may hold values from -6 to 6
- d_attended: bfloat16 [8192, 1024], P('sp', 'tp'), may hold values from -24 to 24
Outputs:
- d_target: bfloat16 [8192, 2048], P('sp')
- d_source: float32 [16384, 2048], P(('sp', 'tp'))
- d_w_query: float32 [2048, 1024], P('sp', 'tp')
All inputs are finite; a program needn't handle non-finite values.
Results may differ from a plain program's by a relative error of at most 0.02.
The roundings to bfloat16 on the way count: a program that leaves them out, or rounds other values in their place, can miss the bound.
Values may be sent and summed in bfloat16 or wider, within the bound.
A program may use at most 64 MiB of HBM per device.

v0:
```python
import jax
import jax.numpy as jnp
from jax import lax
from jax.sharding import Mesh
from jax.sharding import PartitionSpec as P

KVH = 2
HD = 128
SP = ("sp_0", "sp_1")
SP_TP = ("sp_0", "sp_1", "tp")
EPS = 1e-06


def sent_together(arrays, axis, dim, along):
    widths = [a.shape[along] for a in arrays]
    both = jnp.concatenate(arrays, axis=along)
    result = lax.all_gather(both, axis, axis=dim, tiled=True)
    return tuple(jnp.split(result, [sum(widths[:k]) for k in range(1, len(widths))], axis=along))


def joined_all(shard, axes, combine):
    for axis in axes:
        pieces = jax.tree.map(lambda part: lax.all_gather(part, axis), shard)
        shard = jax.tree.map(lambda part: part[0], pieces)
        for k in range(1, lax.axis_size(axis)):
            shard = combine(shard, jax.tree.map(lambda part: part[k], pieces))
    return shard


def in_blocks(shard, dim, peers):
    shape = shard.shape
    pieces = shard.reshape(*shape[:dim], peers, shape[dim] // peers, *shape[dim + 1 :])
    return jnp.moveaxis(pieces, dim, 0)


def sent_and_summed(shard, axis, dim):
    pieces = in_blocks(shard, dim, lax.axis_size(axis))
    arrived = lax.all_to_all(pieces, axis, split_axis=0, concat_axis=0, tiled=True)
    return arrived.sum(axis=0)


def summed_on_arrival(shard, axis, dim):
    peers = lax.axis_size(axis)
    pieces = lax.all_to_all(in_blocks(shard, dim, peers), axis, 0, 0, tiled=True)
    return jnp.sum(pieces.astype(jnp.float32), axis=0)


def joined_along(pieces, dim):
    pieces = jnp.moveaxis(pieces, 0, dim)
    shape = pieces.shape
    return pieces.reshape(*shape[:dim], shape[dim] * shape[dim + 1], *shape[dim + 2 :])


def copy_for_each(shard, axis):
    peers = lax.axis_size(axis)
    return lax.all_to_all(
        jnp.broadcast_to(shard[None], (peers, *shard.shape)), axis, 0, 0, tiled=True
    )


def gathered_copies(shard, axis, dim):
    return joined_along(copy_for_each(shard, axis), dim)


def norm_rows(matrix, gain_vector):
    widened = matrix.astype(jnp.float32)
    inverse = lax.rsqrt(jnp.mean(widened * widened, axis=-1, keepdims=True) + EPS)
    return widened * inverse * gain_vector


def norm_back(matrix, gain_vector, cotangent):
    _, pullback = jax.vjp(lambda values: norm_rows(values, gain_vector), matrix.astype(jnp.float32))
    return pullback(cotangent)[0]


def block_count(row_count, most_rows):
    number = 1
    while row_count % (number * 2) == 0 and row_count // number > most_rows:
        number = number * 2
    return number


def merge_totals(earlier, latter):
    maxima = jnp.maximum(earlier[0], latter[0])
    totals = earlier[1] * jnp.exp(earlier[0] - maxima) + latter[1] * jnp.exp(latter[0] - maxima)
    return (maxima, totals)


def block_totals(queries, key_head, scaling):
    row_count = queries.shape[0]
    per_head = queries.reshape(row_count, -1, key_head.shape[1])
    scores = (
        jnp.einsum("rhd,sd->rhs", per_head, key_head, preferred_element_type=jnp.float32) * scaling
    )
    maxima = jnp.max(scores, axis=-1)
    totals = jnp.sum(jnp.exp(scores - maxima[..., None]), axis=-1)
    return (maxima, totals)


def score_grads(query_heads, grad_heads, delta_rows, log_total, key_head, value_head, scaling):
    scores = (
        jnp.einsum("rhd,sd->rhs", query_heads, key_head, preferred_element_type=jnp.float32)
        * scaling
    )
    weights = jnp.exp(scores - log_total[..., None])
    d_weights = jnp.einsum(
        "rhd,sd->rhs", grad_heads, value_head, preferred_element_type=jnp.float32
    )
    d_scores = (weights * (d_weights - delta_rows.astype(jnp.float32)[..., None])).astype(
        jnp.bfloat16
    )
    return (weights, d_scores)


def gradient_block(carried, blocks, key_head, value_head, scaling):
    key_acc, value_acc = carried
    queries, cotangent, delta_rows, log_total = blocks
    row_count = queries.shape[0]
    head_dim = key_head.shape[1]
    query_heads = queries.reshape(row_count, -1, head_dim)
    grad_heads = cotangent.reshape(row_count, -1, head_dim)
    weights, d_scores = score_grads(
        query_heads, grad_heads, delta_rows, log_total, key_head, value_head, scaling
    )
    key_acc = (
        key_acc
        + jnp.einsum("rhs,rhd->sd", d_scores, query_heads, preferred_element_type=jnp.float32)
        * scaling
    )
    value_acc = value_acc + jnp.einsum(
        "rhs,rhd->sd", weights.astype(jnp.bfloat16), grad_heads, preferred_element_type=jnp.float32
    )
    return ((key_acc, value_acc), None)


def local(target, source, target_gain, source_gain, w_query, w_key, w_value, attended, d_attended):
    tp_size = lax.axis_size("tp")
    local_rows = target.shape[0]
    source_rows = source.shape[0]
    query_width = w_query.shape[1]
    scaling = HD ** (-0.5)
    normed_target = norm_rows(target, target_gain).astype(jnp.bfloat16)
    normed_source = norm_rows(source, source_gain).astype(jnp.bfloat16)
    query = jnp.dot(normed_target, w_query, preferred_element_type=jnp.float32).astype(jnp.bfloat16)
    key_own = jnp.dot(normed_source, w_key, preferred_element_type=jnp.float32).astype(jnp.bfloat16)
    value_own = jnp.dot(normed_source, w_value, preferred_element_type=jnp.float32).astype(
        jnp.bfloat16
    )
    key_block, value_block = sent_together((key_own, value_own), "tp", 0, 1)
    group_size = tp_size // KVH
    kv_index = lax.axis_index("tp") // group_size
    key_head = lax.dynamic_slice_in_dim(key_block, kv_index * HD, HD, 1)
    value_head = lax.dynamic_slice_in_dim(value_block, kv_index * HD, HD, 1)
    delta = jnp.einsum(
        "rhd,rhd->rh",
        d_attended.reshape(local_rows, -1, HD),
        attended.reshape(local_rows, -1, HD),
        preferred_element_type=jnp.float32,
    ).astype(jnp.bfloat16)
    all_queries = lax.all_gather(query, SP, axis=0, tiled=True)
    target_total = all_queries.shape[0]
    number = block_count(target_total, 512)
    maxima, totals = lax.map(
        lambda blocked: block_totals(blocked, key_head, scaling),
        all_queries.reshape(number, target_total // number, query_width),
    )
    maxima = maxima.reshape(target_total, -1)
    totals = totals.reshape(target_total, -1)
    maxima, totals = joined_all((maxima, totals), SP, merge_totals)
    log_total = maxima + jnp.log(totals)
    block_rows = key_head.shape[0]
    start_state = (
        jnp.zeros((block_rows, HD), jnp.float32),
        jnp.zeros((block_rows, HD), jnp.float32),
    )
    key_acc = start_state[0]
    value_acc = start_state[1]
    cotangent, delta_piece = sent_together((d_attended, delta), SP, 0, 1)
    row_count = cotangent.shape[0]
    pieces_count = block_count(row_count, 512)
    blocked = tuple(
        (
            member.reshape((pieces_count, row_count // pieces_count) + member.shape[1:])
            for member in (all_queries, cotangent, delta_piece, log_total)
        )
    )

    def fold_inner_step(state, blocks):
        return gradient_block(state, blocks, key_head, value_head, scaling)

    (key_acc, value_acc), grad_rows = lax.scan(fold_inner_step, (key_acc, value_acc), blocked)
    folded = (key_acc, value_acc)
    key_acc = folded[0]
    value_acc = folded[1]
    own_totals = lax.dynamic_slice_in_dim(log_total, lax.axis_index(SP) * local_rows, local_rows, 0)
    own_queries = query.reshape(local_rows, -1, HD)
    own_grads = d_attended.reshape(local_rows, -1, HD)
    query_start = jnp.zeros((local_rows, query_width // HD, HD), jnp.float32)
    keys_piece, values_piece = sent_together((key_head, value_head), SP, 0, 1)
    row_count = keys_piece.shape[0]
    pieces_count = block_count(row_count, 512)
    key_blocks = keys_piece.reshape(pieces_count, row_count // pieces_count, HD)
    value_blocks = values_piece.reshape(pieces_count, row_count // pieces_count, HD)

    def key_inner_step(state, blocks):
        keys_now, values_now = blocks
        _, d_scores = score_grads(
            own_queries, own_grads, delta, own_totals, keys_now, values_now, scaling
        )
        return (
            state
            + jnp.einsum("rhs,sd->rhd", d_scores, keys_now, preferred_element_type=jnp.float32)
            * scaling,
            None,
        )

    result, _ = lax.scan(key_inner_step, query_start, (key_blocks, value_blocks))
    d_query = result.reshape(local_rows, query_width).astype(jnp.bfloat16)
    d_w_query = sent_and_summed(
        jnp.einsum("rd,rc->dc", normed_target, d_query, preferred_element_type=jnp.float32), SP, 0
    )
    share_rows = local_rows // tp_size
    grad_rows = d_query
    d_normed = summed_on_arrival(
        jnp.einsum("rc,dc->rd", grad_rows, w_query, preferred_element_type=jnp.float32).astype(
            jnp.bfloat16
        ),
        "tp",
        0,
    )
    own_rows = lax.dynamic_slice_in_dim(target, lax.axis_index("tp") * share_rows, share_rows, 0)
    own_grad = norm_back(own_rows, target_gain, d_normed).astype(jnp.bfloat16)
    d_target = gathered_copies(own_grad, "tp", 0)
    stacked = jnp.stack([key_acc, value_acc], axis=1).reshape(tp_size, source_rows, 2 * HD)
    returned = lax.all_to_all(
        stacked.astype(jnp.bfloat16), "tp", split_axis=0, concat_axis=0, tiled=True
    ).astype(stacked.dtype)
    grouped = returned.reshape(KVH, group_size, source_rows, 2, HD).sum(axis=1)
    d_key = (
        grouped[:, :, 0, :].transpose(1, 0, 2).reshape(source_rows, KVH * HD).astype(jnp.bfloat16)
    )
    d_value = (
        grouped[:, :, 1, :].transpose(1, 0, 2).reshape(source_rows, KVH * HD).astype(jnp.bfloat16)
    )
    d_normed_source = jnp.einsum(
        "rc,dc->rd", d_key, w_key, preferred_element_type=jnp.float32
    ) + jnp.einsum("rc,dc->rd", d_value, w_value, preferred_element_type=jnp.float32)
    d_source = norm_back(source, source_gain, d_normed_source)
    return (d_target, d_source, d_w_query)


def solution(mesh):
    finer = Mesh(mesh.devices.reshape(16, 4, mesh.shape["tp"]), ("sp_0", "sp_1", "tp"))
    placed = (
        P(SP, None),
        P(SP_TP, None),
        P(),
        P(),
        P(None, "tp"),
        P(),
        P(),
        P(SP, "tp"),
        P(SP, "tp"),
    )
    return jax.shard_map(
        local,
        mesh=finer,
        in_specs=placed,
        out_specs=(P(SP, None), P(SP_TP, None), P(SP, "tp")),
        check_vma=False,
    )
```

profile of v0, /device:TPU:8, one launch (start us, length us, event | category | flops | bytes accessed | tf_op | source)
XLA Modules:
  0.0 659.4 jit_solution(8378921525425368850)
XLA Ops:
  7.3 1.5 copy.20
  10.1 2.0 convolution_convert_fusion.1
  17.0 13.2 %all_gather.26 = bf16[256,512]{1,0:T(8,128)(2,1)S(1)} all-gather(bf16[32,512]{1,0:T(8,128)(2,1)S(1)} %pad_maximum_fusion.3), channel_id=1, replica_groups=mesh['sp_0'=16,'sp_1'=4,'tp'=8] {'tp'}, dimensions={0}, use_global_device_ids=true | all-gather | bytes 294912 | tf_op jit(solution)/shard_map/all_gather | solution.py:17
  31.0 125.5 %all-gather.6.cloned.1.call-done = bf16[8192,128]{1,0:T(8,128)(2,1)} async-done(((bf16[128,128]{1,0:T(8,128)(2,1)}), bf16[8192,128]{1,0:T(8,128)(2,1)}) %all-gather.6.cloned.1.call-update) | async-done | bytes 2097168 | tf_op jit(solution)/shard_map/all_gather | solution.py:160
  156.5 20.6 %while.36 = (s32[]{:T(128)}, f32[16,512,1]{1,2,0:T(1,128)S(1)}, f32[16,512,1]{1,2,0:T(1,128)S(1)}, bf16[16,512,128]{2,1,0:T(8,128)(2,1)}, bf16[256,128]{1,0:T(8,128)(2,1)S(1)}, /*index=5*/s32[]{:T(128)}) while((s32[]{:T(128)}, f32[16,512,1]{1,2,0:T(1,128)S(1)}, f32[16,512,1]{1,2,0:T(1,128)S(1)}, bf16[16,512,128]{2,1,0:T(8,128)(2,1)}, ...), condition=%wide.region_5.6_spmd, body=%wide.region_2.5_spmd.sunk | while | flops 34077696 | bytes 1259605 | solution.py:163
  177.1 31.7 %all_gather.31 = f32[16,8192,1]{1,2,0:T(1,128)S(1)} all-gather(f32[1,8192,1]{1,2,0:T(1,128)S(1)} %bitcast.234), channel_id=1, replica_groups=mesh['sp_0'=16,'sp_1'=4,'tp'=8] {'sp_0'}, dimensions={0}, use_global_device_ids=true | all-gather | bytes 557056 | tf_op jit(solution)/shard_map/all_gather | solution.py:23
  208.8 29.3 %all_gather.29 = f32[16,8192,1]{1,2,0:T(1,128)S(1)} all-gather(f32[1,8192,1]{1,2,0:T(1,128)} %bitcast.233), channel_id=1, replica_groups=mesh['sp_0'=16,'sp_1'=4,'tp'=8] {'sp_0'}, dimensions={0}, use_global_device_ids=true | all-gather | bytes 557056 | tf_op jit(solution)/shard_map/all_gather | solution.py:23
  239.6 12.6 %all_gather.30 = f32[4,8192,1]{1,2,0:T(1,128)S(1)} all-gather(f32[1,8192,1]{1,2,0:T(1,128)S(1)} %get-tuple-element.240), channel_id=1, replica_groups=mesh['sp_0'=16,'sp_1'=4,'tp'=8] {'sp_1'}, dimensions={0}, use_global_device_ids=true | all-gather | bytes 163840 | tf_op jit(solution)/shard_map/all_gather | solution.py:23
  252.3 12.1 %all_gather.32 = f32[4,8192,1]{1,2,0:T(1,128)S(1)} all-gather(f32[1,8192,1]{1,2,0:T(1,128)S(1)} %get-tuple-element.239), channel_id=1, replica_groups=mesh['sp_0'=16,'sp_1'=4,'tp'=8] {'sp_1'}, dimensions={0}, use_global_device_ids=true | all-gather | bytes 163840 | tf_op jit(solution)/shard_map/all_gather | solution.py:23
  265.3 36.0 %all-gather.8.cloned.1.call-done = bf16[8192,129]{1,0:T(8,128)(2,1)} async-done(((bf16[128,129]{1,0:T(8,128)(2,1)}), bf16[8192,129]{1,0:T(8,128)(2,1)}) %all-gather.8.cloned.1.call-update) | async-done | bytes 2113552 | tf_op jit(solution)/shard_map/all_gather | solution.py:17
  301.3 2.2 slice_reduce_fusion
  304.1 3.0 split.28
  307.2 84.5 %while.38 = (s32[]{:T(128)}, f32[256,128]{1,0:T(8,128)S(1)}, f32[256,128]{1,0:T(8,128)S(1)}, bf16[16,512,128]{2,1,0:T(8,128)(2,1)}, bf16[256,128]{1,0:T(8,128)(2...) while((s32[]{:T(128)}, f32[256,128]{1,0:T(8,128)S(1)}, ...), condition=%wide.region_12.13_spmd.clone, body=%wide.region_11.12_spmd.clone.sunk | while | flops 135168512 | bytes 2765455 | solution.py:191
  309.7 1.5 fusion.176
  315.0 1.5 fusion.176
  320.3 1.5 fusion.176
  325.5 1.5 fusion.176
  330.8 1.5 fusion.176
  336.1 1.5 fusion.176
  341.4 1.5 fusion.176
  346.7 1.5 fusion.176
  351.9 1.5 fusion.176
  357.2 1.5 fusion.176
  362.5 1.5 fusion.176
  367.8 1.5 fusion.176
  373.1 1.5 fusion.176
  378.3 1.5 fusion.176
  383.6 1.5 fusion.176
  389.0 1.5 fusion.176
  391.7 64.3 %all-gather.4.cloned.1.call-done = bf16[16384,256]{1,0:T(8,128)(2,1)} async-done(((bf16[256,256]{1,0:T(8,128)(2,1)}), bf16[16384,256]{1,0:T(8,128)(2,1)}) %all-gather.4.cloned.1.call-update) | async-done | bytes 8388624 | tf_op jit(solution)/shard_map/all_gather | solution.py:17
  456.0 5.7 fusion.125
  461.8 81.4 %while.37 = (s32[]{:T(128)}, f32[128,1,128]{2,0,1:T(8,128)S(1)}, bf16[32,512,128]{2,1,0:T(8,128)(2,1)}, bf16[128,1,128]{2,0,1:T(8,128)(2,1)S(1)}, f32[128,1]{0,1...) while((s32[]{:T(128)}, f32[128,1,128]{2,0,1:T(8,128)S(1)}, ...), condition=%wide.region_7.8_spmd.clone, body=%wide.region_6.7_spmd.clone.sunk | while | flops 50708608 | bytes 1117562 | solution.py:217
  462.9 1.4 fusion.167
  465.5 1.4 fusion.167
  468.0 1.4 fusion.167
  473.1 1.4 fusion.167
  475.6 1.4 fusion.167
  478.2 1.4 fusion.167
  543.2 2.1 convolution_convert_fusion
  545.3 4.3 all-to-all-start
  550.5 9.5 %all-to-all-done = bf16[8,16,2048]{2,1,0:T(8,128)(2,1)} async-done(((bf16[8,16,2048]{2,1,0:T(8,128)(2,1)}), bf16[8,16,2048]{2,1,0:T(8,128)(2,1)}, u32[]{:S(2)}, u32[]{:S(2)}) %all-to-all-start) | async-done | bytes 524320 | tf_op jit(solution)/shard_map/all_to_all | solution.py:44
  560.0 3.4 all-to-all-start.2
  566.5 2.9 all-to-all-done.2
  570.2 4.3 all-to-all-start.1
  575.8 9.1 %all-to-all-done.1 = bf16[8,16,2048]{2,1,0:T(8,128)(2,1)} async-done(((bf16[8,16,2048]{2,1,0:T(8,128)(2,1)}), bf16[8,16,2048]{2,1,0:T(8,128)(2,1)}, u32[]{:S(2)}, u32[]{:S(2)}) %all-to-all-start.1) | async-done | bytes 524320 | tf_op jit(solution)/shard_map/all_to_all | solution.py:56
  584.9 10.6 %all-to-all-start.3 = ((f32[64,32,128]{2,1,0:T(8,128)}), f32[64,32,128]{2,1,0:T(8,128)S(1)}, u32[]{:S(2)}, u32[]{:S(2)}) async-start(f32[64,32,128]{2,1,0:T(8,128)} %fusion.92), calls=%async_computation.3 | async-start | bytes 2097152 | tf_op jit(solution)/shard_map/all_to_all | solution.py:38
  598.4 51.9 %all-to-all-done.3 = f32[64,32,128]{2,1,0:T(8,128)S(1)} async-done(((f32[64,32,128]{2,1,0:T(8,128)}), f32[64,32,128]{2,1,0:T(8,128)S(1)}, u32[]{:S(2)}, u32[]{:S(2)}) %all-to-all-start.3) | async-done | bytes 1048608 | tf_op jit(solution)/shard_map/all_to_all | solution.py:38
  651.0 1.9 copy.89
  (289 shorter events, 171.6 us)
Async XLA Ops:
  7.2 9.1 %copy-start = (bf16[2048,256]{1,0:T(8,128)(2,1)S(1)}, bf16[2048,256]{1,0:T(8,128)(2,1)}, u32[]{:S(2)}) copy-start(bf16[2048,256]{1,0:T(8,128)(2,1)} %param.21) | copy-start | bytes 3145732
  7.2 9.1 %copy-start.2 = (bf16[32,2048]{1,0:T(8,128)(2,1)S(1)}, bf16[32,2048]{1,0:T(8,128)(2,1)}, u32[]{:S(2)}) copy-start(bf16[32,2048]{1,0:T(8,128)(2,1)} %param.16) | copy-start | bytes 393220
  7.2 9.1 %copy-start.8 = (f32[2048]{0:T(1024)S(1)}, f32[2048]{0:T(1024)}, u32[]{:S(2)}) copy-start(f32[2048]{0:T(1024)} %param.18) | copy-start | bytes 24580
  7.2 9.4 %copy-start.1 = (bf16[2048,256]{1,0:T(8,128)(2,1)S(1)}, bf16[2048,256]{1,0:T(8,128)(2,1)}, u32[]{:S(2)}) copy-start(bf16[2048,256]{1,0:T(8,128)(2,1)} %param.20) | copy-start | bytes 3145732
  7.2 149.3 %all-gather.6.cloned.1.call-start = ((), (), s32[]{:S(2)}) async-start(), calls=%async_computation.5 | async-start | bytes 2129920 | tf_op jit(solution)/shard_map/all_gather | solution.py:160
  12.1 289.2 %all-gather.8.cloned.1.call-start = ((), (), s32[]{:S(2)}) async-start(), calls=%async_computation.6 | async-start | bytes 4259840 | tf_op jit(solution)/shard_map/all_gather | solution.py:17
  13.0 2.7 copy-start.13
  14.6 441.5 %all-gather.4.cloned.1.call-start = ((), (), s32[]{:S(2)}) async-start(), calls=%async_computation.4 | async-start | bytes 8519680 | tf_op jit(solution)/shard_map/all_gather | solution.py:17
  15.7 0.6 copy-start.15
  16.3 13.9 %copy-start.11 = (f32[32]{0:T(128)}, f32[32]{0:T(128)S(1)}, u32[]{:S(2)}) copy-start(f32[32]{0:T(128)S(1)} %fusion.122) | copy-start | bytes 388
  177.1 31.8 %copy-start.10 = (f32[16,512,1]{1,2,0:T(1,128)}, f32[16,512,1]{1,2,0:T(1,128)S(1)}, u32[]{:S(2)}) copy-start(f32[16,512,1]{1,2,0:T(1,128)S(1)} %get-tuple-element.121) | copy-start | bytes 98308
  391.7 70.1 %copy-start.4 = (f32[128,1,128]{2,0,1:T(8,128)S(1)}, f32[128,1,128]{2,0,1:T(8,128)}, u32[]{:S(2)}) copy-start(f32[128,1,128]{2,0,1:T(8,128)} %custom-call) | copy-start | bytes 196612
  391.7 70.0 %copy-start.5 = (bf16[128,128]{1,0:T(8,128)(2,1)S(1)}, bf16[128,128]{1,0:T(8,128)(2,1)}, u32[]{:S(2)}) copy-start(bf16[128,128]{1,0:T(8,128)(2,1)} %convolution_convert_fusion.1) | copy-start | bytes 98308
  391.7 70.0 %copy-start.6 = (bf16[128,128]{1,0:T(8,128)(2,1)S(1)}, bf16[128,128]{1,0:T(8,128)(2,1)}, u32[]{:S(2)}) copy-start(bf16[128,128]{1,0:T(8,128)(2,1)} %param.23) | copy-start | bytes 98308
  391.7 70.0 %copy-start.14 = (bf16[128]{0:T(256)(128)(2,1)S(1)}, bf16[128]{0:T(256)(128)(2,1)}, u32[]{:S(2)}) copy-start(bf16[128]{0:T(256)(128)(2,1)} %copy-done.13) | copy-start | bytes 772
  461.8 102.8 %copy-start.9 = (f32[2048]{0:T(1024)S(1)}, f32[2048]{0:T(1024)}, u32[]{:S(2)}) copy-start(f32[2048]{0:T(1024)} %param.17) | copy-start | bytes 24580
  545.3 14.7 %all-to-all-start = ((bf16[8,16,2048]{2,1,0:T(8,128)(2,1)}), bf16[8,16,2048]{2,1,0:T(8,128)(2,1)}, u32[]{:S(2)}, u32[]{:S(2)}) async-start(bf16[8,16,2048]{2,1,0:T(8,128)(2,1)} %bitcast.217), calls=%async_computation | async-start | bytes 1048576 | tf_op jit(solution)/shard_map/all_to_all | solution.py:44
  560.0 9.4 %all-to-all-start.2 = ((bf16[8,32,256]{2,1,0:T(8,128)(2,1)}), bf16[8,32,256]{2,1,0:T(8,128)(2,1)S(1)}, u32[]{:S(2)}, u32[]{:S(2)}) async-start(bf16[8,32,256]{2,1,0:T(8,128)(2,1)} %convert_element_type.121), calls=%async_computation.2 | async-start | bytes 262144 | tf_op jit(solution)/shard_map/all_to_all | solution.py:235
  563.4 33.6 %copy-start.3 = (bf16[32,2048]{1,0:T(8,128)(2,1)S(1)}, bf16[32,2048]{1,0:T(8,128)(2,1)}, u32[]{:S(2)}) copy-start(bf16[32,2048]{1,0:T(8,128)(2,1)} %param.16) | copy-start | bytes 393220
  569.4 15.5 %copy-start.7 = (bf16[8,32,256]{2,1,0:T(8,128)(2,1)}, bf16[8,32,256]{2,1,0:T(8,128)(2,1)S(1)}, u32[]{:S(2)}) copy-start(bf16[8,32,256]{2,1,0:T(8,128)(2,1)S(1)} %all-to-all-done.2) | copy-start | bytes 393220
  570.2 27.3 %copy-start.16 = (f32[32]{0:T(128)S(1)}, f32[32]{0:T(128)}, u32[]{:S(2)}) copy-start(f32[32]{0:T(128)} %copy-done.15) | copy-start | bytes 388
  570.2 27.3 %copy-start.12 = (f32[32]{0:T(128)S(1)}, f32[32]{0:T(128)}, u32[]{:S(2)}) copy-start(f32[32]{0:T(128)} %copy-done.11) | copy-start | bytes 388
  570.2 14.6 %all-to-all-start.1 = ((bf16[8,16,2048]{2,1,0:T(8,128)(2,1)}), bf16[8,16,2048]{2,1,0:T(8,128)(2,1)}, u32[]{:S(2)}, u32[]{:S(2)}) async-start(bf16[8,16,2048]{2,1,0:T(8,128)(2,1)} %broadcast_in_dim.22), calls=%async_computation.1 | async-start | bytes 1048576 | tf_op jit(solution)/shard_map/all_to_all | solution.py:56
  584.9 65.5 %all-to-all-start.3 = ((f32[64,32,128]{2,1,0:T(8,128)}), f32[64,32,128]{2,1,0:T(8,128)S(1)}, u32[]{:S(2)}, u32[]{:S(2)}) async-start(f32[64,32,128]{2,1,0:T(8,128)} %fusion.92), calls=%async_computation.3 | async-start | bytes 2097152 | tf_op jit(solution)/shard_map/all_to_all | solution.py:38
Sparse Core Ops, SparseCore 0:
  12.2 144.2 all-gather.5
  159.4 141.8 all-gather.7
  304.8 151.1 all-gather.3
where the time goes:
time: 664 us; the launch traced here: 659 us
  waiting for transfers between devices  299 us (45%)
  matrix products  167 us (25%)
  blocking collectives  98.9 us (15%)
  local copies, waits for them, and re-layouts  29.6 us (4%)
  other arithmetic  25.7 us (4%)
  starting transfers between devices  22.6 us (3%)
  between operations  14.2 us (2%)
    all_gather x1, waiting for transfers between devices, local(): all_queries = lax.all_gather(query, SP, axis=0, tiled=True)  125 us
    all_gather x2, waiting for transfers between devices, sent_together(): result = lax.all_gather(both, axis, axis=dim, tiled=True)  100 us
    all_gather x4, blocking collectives, joined_all(): pieces = jax.tree.map(lambda part: lax.all_gather(part, axis), shard)  85.7 us
    dot_general x48, matrix products, score_grads(): jnp.einsum('rhd,sd->rhs', query_heads, key_head, preferred_element_type=j...  53.8 us
    all_to_all x1, waiting for transfers between devices, sent_and_summed(): lax.all_to_all(pieces, axis, split_axis=0, concat_axis=0, tiled=True)  51.9 us
    dot_general x32, matrix products, key_inner_step(): jnp.einsum('rhs,sd->rhd', d_scores, keys_now, preferred_element_type=jnp....  44.5 us
    dot_general x16, matrix products, gradient_block(): jnp.einsum('rhs,rhd->sd', d_scores, query_heads, preferred_element_type=j...  24.1 us
    dot_general x16, matrix products, gradient_block(): jnp.einsum('rhs,rhd->sd', weights.astype(jnp.bfloat16), grad_heads, prefe...  19.2 us
  transfers between devices with their start and end apart: 7, of which 7 were waited for; matrix products, arithmetic and copies ran while one was open for 19% of the time, Pallas kernels for 0%

commit v1 on v0

--- a/solution.py
+++ b/solution.py
@@ -157,7 +157,9 @@
         attended.reshape(local_rows, -1, HD),
         preferred_element_type=jnp.float32,
     ).astype(jnp.bfloat16)
-    all_queries = lax.all_gather(query, SP, axis=0, tiled=True)
+    all_queries = jnp.concatenate(
+        lax.all_to_all(jnp.stack([query] * lax.axis_size(SP)), SP, 0, 0), axis=0
+    )
     target_total = all_queries.shape[0]
     number = block_count(target_total, 512)
     maxima, totals = lax.map(

time: 664 us -> 608 us (0.916)
  waiting for transfers between devices: 299 us -> 222 us
  starting transfers between devices: 22.6 us -> 41.8 us
    all_gather x1 -> x0, waiting for transfers between devices: 125 us -> none  [local(): all_queries = lax.all_gather(query, SP, axis=0, tiled=True)]
    all_gather x2, waiting for transfers between devices: 100 us -> 149 us  [sent_together(): result = lax.all_gather(both, axis, axis=dim, tiled=True)]
    all_to_all x0 -> x1, starting transfers between devices: none -> 18.9 us  [local(): lax.all_to_all(jnp.stack([query] * lax.axis_size(SP)), SP, 0, 0)]
  transfers between devices with their start and end apart: 7 -> 7, of which waited for: 7 -> 5; matrix products, arithmetic and copies ran while one was open for 19% -> 20% of each run, Pallas kernels for 0% -> 0%
where the time goes in v1:
time: 608 us; the launch traced here: 604 us
  waiting for transfers between devices  222 us (37%)
  matrix products  166 us (27%)
  blocking collectives  101 us (17%)
  starting transfers between devices  41.8 us (7%)
  local copies, waits for them, and re-layouts  32 us (5%)
  other arithmetic  23.3 us (4%)
  between operations  14.5 us (2%)
    all_gather x2, waiting for transfers between devices, sent_together(): result = lax.all_gather(both, axis, axis=dim, tiled=True)  149 us
    all_gather x4, blocking collectives, joined_all(): pieces = jax.tree.map(lambda part: lax.all_gather(part, axis), shard)  87.6 us
    dot_general x48, matrix products, score_grads(): jnp.einsum('rhd,sd->rhs', query_heads, key_head, preferred_element_type=j...  53.7 us
    all_to_all x1, waiting for transfers between devices, sent_and_summed(): lax.all_to_all(pieces, axis, split_axis=0, concat_axis=0, tiled=True)  51.9 us
    dot_general x32, matrix products, key_inner_step(): jnp.einsum('rhs,sd->rhd', d_scores, keys_now, preferred_element_type=jnp....  44.5 us
    dot_general x16, matrix products, gradient_block(): jnp.einsum('rhs,rhd->sd', d_scores, query_heads, preferred_element_type=j...  24.1 us
    dot_general x16, matrix products, gradient_block(): jnp.einsum('rhs,rhd->sd', weights.astype(jnp.bfloat16), grad_heads, prefe...  19.2 us
    all_to_all x1, starting transfers between devices, local(): lax.all_to_all(jnp.stack([query] * lax.axis_size(SP)), SP, 0, 0)  18.9 us
  transfers between devices with their start and end apart: 7, of which 5 were waited for; matrix products, arithmetic and copies ran while one was open for 20% of the time, Pallas kernels for 0%

profile of v1, /device:TPU:8, one launch (start us, length us, event | category | flops | bytes accessed | tf_op | source)
XLA Modules:
  0.0 603.5 jit_solution(10714220270812947956)
XLA Ops:
  7.2 1.4 copy.20
  12.0 1.8 stack.11
  13.8 18.9 %all-to-all-start = ((bf16[64,128,128]{2,1,0:T(8,128)(2,1)}), bf16[64,128,128]{2,1,0:T(8,128)(2,1)}, u32[]{:S(2)}, u32[]{:S(2)}) async-start(bf16[64,128,128]{2,1,0:T(8,128)(2,1)} %stack.11), calls=%async_computation | async-start | bytes 4194304 | tf_op jit(solution)/shard_map/all_to_all | solution.py:161
  35.3 13.2 %all_gather.23 = bf16[256,512]{1,0:T(8,128)(2,1)S(1)} all-gather(bf16[32,512]{1,0:T(8,128)(2,1)S(1)} %pad_maximum_fusion.3), channel_id=1, replica_groups=mesh['sp_0'=16,'sp_1'=4,'tp'=8] {'tp'}, dimensions={0}, use_global_device_ids=true | all-gather | bytes 294912 | tf_op jit(solution)/shard_map/all_gather | solution.py:17
  49.3 149.0 %all-gather.5.cloned.1.call-done = bf16[8192,129]{1,0:T(8,128)(2,1)} async-done(((bf16[128,129]{1,0:T(8,128)(2,1)}), bf16[8192,129]{1,0:T(8,128)(2,1)}) %all-gather.5.cloned.1.call-update) | async-done | bytes 2113552 | tf_op jit(solution)/shard_map/all_gather | solution.py:17
  198.3 2.2 slice_reduce_fusion
  201.2 3.0 split.28
  204.2 20.6 %while.36 = (s32[]{:T(128)}, f32[16,512,1]{1,2,0:T(1,128)S(1)}, f32[16,512,1]{1,2,0:T(1,128)S(1)}, bf16[16,512,128]{2,1,0:T(8,128)(2,1)}, bf16[256,128]{1,0:T(8,128)(2,1)S(1)}, /*index=5*/s32[]{:T(128)}) while((s32[]{:T(128)}, f32[16,512,1]{1,2,0:T(1,128)S(1)}, f32[16,512,1]{1,2,0:T(1,128)S(1)}, bf16[16,512,128]{2,1,0:T(8,128)(2,1)}, ...), condition=%wide.region_5.6_spmd, body=%wide.region_2.5_spmd.sunk | while | flops 34077696 | bytes 1259605 | solution.py:165
  224.8 32.4 %all_gather.27 = f32[16,8192,1]{1,2,0:T(1,128)S(1)} all-gather(f32[1,8192,1]{1,2,0:T(1,128)S(1)} %bitcast.233), channel_id=1, replica_groups=mesh['sp_0'=16,'sp_1'=4,'tp'=8] {'sp_0'}, dimensions={0}, use_global_device_ids=true | all-gather | bytes 557056 | tf_op jit(solution)/shard_map/all_gather | solution.py:23
  257.2 30.1 %all_gather.25 = f32[16,8192,1]{1,2,0:T(1,128)S(1)} all-gather(f32[1,8192,1]{1,2,0:T(1,128)} %bitcast.232), channel_id=1, replica_groups=mesh['sp_0'=16,'sp_1'=4,'tp'=8] {'sp_0'}, dimensions={0}, use_global_device_ids=true | all-gather | bytes 557056 | tf_op jit(solution)/shard_map/all_gather | solution.py:23
  288.8 12.6 %all_gather.26 = f32[4,8192,1]{1,2,0:T(1,128)S(1)} all-gather(f32[1,8192,1]{1,2,0:T(1,128)S(1)} %get-tuple-element.240), channel_id=1, replica_groups=mesh['sp_0'=16,'sp_1'=4,'tp'=8] {'sp_1'}, dimensions={0}, use_global_device_ids=true | all-gather | bytes 163840 | tf_op jit(solution)/shard_map/all_gather | solution.py:23
  301.5 12.5 %all_gather.28 = f32[4,8192,1]{1,2,0:T(1,128)S(1)} all-gather(f32[1,8192,1]{1,2,0:T(1,128)S(1)} %get-tuple-element.239), channel_id=1, replica_groups=mesh['sp_0'=16,'sp_1'=4,'tp'=8] {'sp_1'}, dimensions={0}, use_global_device_ids=true | all-gather | bytes 163840 | tf_op jit(solution)/shard_map/all_gather | solution.py:23
  314.9 84.5 %while.38 = (s32[]{:T(128)}, f32[256,128]{1,0:T(8,128)S(1)}, f32[256,128]{1,0:T(8,128)S(1)}, bf16[16,512,128]{2,1,0:T(8,128)(2,1)}, bf16[256,128]{1,0:T(8,128)(2...) while((s32[]{:T(128)}, f32[256,128]{1,0:T(8,128)S(1)}, ...), condition=%wide.region_12.13_spmd.clone, body=%wide.region_11.12_spmd.clone.sunk | while | flops 135168512 | bytes 2765455 | solution.py:193
  317.5 1.5 fusion.176
  322.8 1.5 fusion.176
  328.1 1.5 fusion.176
  333.4 1.5 fusion.176
  338.6 1.5 fusion.176
  343.9 1.5 fusion.176
  349.2 1.5 fusion.176
  354.5 1.5 fusion.176
  359.7 1.5 fusion.176
  365.0 1.5 fusion.176
  370.3 1.5 fusion.176
  375.6 1.5 fusion.176
  380.9 1.5 fusion.176
  386.1 1.5 fusion.176
  391.4 1.5 fusion.176
  396.7 1.5 fusion.176
  399.5 5.7 fusion.125
  405.3 81.4 %while.37 = (s32[]{:T(128)}, f32[128,1,128]{2,0,1:T(8,128)S(1)}, bf16[32,512,128]{2,1,0:T(8,128)(2,1)}, bf16[128,1,128]{2,0,1:T(8,128)(2,1)S(1)}, f32[128,1]{0,1...) while((s32[]{:T(128)}, f32[128,1,128]{2,0,1:T(8,128)S(1)}, ...), condition=%wide.region_7.8_spmd.clone, body=%wide.region_6.7_spmd.clone.sunk | while | flops 50708608 | bytes 1117562 | solution.py:219
  406.4 1.4 fusion.167
  408.9 1.4 fusion.167
  411.5 1.4 fusion.167
  414.0 1.4 fusion.167
  416.6 1.4 fusion.167
  419.1 1.4 fusion.167
  421.7 1.4 fusion.167
  486.6 2.1 convolution_convert_fusion
  488.8 4.2 all-to-all-start.1
  493.9 9.5 %all-to-all-done.1 = bf16[8,16,2048]{2,1,0:T(8,128)(2,1)} async-done(((bf16[8,16,2048]{2,1,0:T(8,128)(2,1)}), bf16[8,16,2048]{2,1,0:T(8,128)(2,1)}, u32[]{:S(2)}, u32[]{:S(2)}) %all-to-all-start.1) | async-done | bytes 524320 | tf_op jit(solution)/shard_map/all_to_all | solution.py:44
  503.4 3.4 all-to-all-start.3
  509.9 2.9 all-to-all-done.3
  513.6 4.3 all-to-all-start.2
  519.2 9.1 %all-to-all-done.2 = bf16[8,16,2048]{2,1,0:T(8,128)(2,1)} async-done(((bf16[8,16,2048]{2,1,0:T(8,128)(2,1)}), bf16[8,16,2048]{2,1,0:T(8,128)(2,1)}, u32[]{:S(2)}, u32[]{:S(2)}) %all-to-all-start.2) | async-done | bytes 524320 | tf_op jit(solution)/shard_map/all_to_all | solution.py:56
  528.3 11.0 %all-to-all-start.4 = ((f32[64,32,128]{2,1,0:T(8,128)}), f32[64,32,128]{2,1,0:T(8,128)S(1)}, u32[]{:S(2)}, u32[]{:S(2)}) async-start(f32[64,32,128]{2,1,0:T(8,128)} %fusion.92), calls=%async_computation.4 | async-start | bytes 2097152 | tf_op jit(solution)/shard_map/all_to_all | solution.py:38
  542.2 51.9 %all-to-all-done.4 = f32[64,32,128]{2,1,0:T(8,128)S(1)} async-done(((f32[64,32,128]{2,1,0:T(8,128)}), f32[64,32,128]{2,1,0:T(8,128)S(1)}, u32[]{:S(2)}, u32[]{:S(2)}) %all-to-all-start.4) | async-done | bytes 1048608 | tf_op jit(solution)/shard_map/all_to_all | solution.py:38
  594.8 1.9 copy.89
  (295 shorter events, 169.7 us)
Async XLA Ops:
  7.2 27.4 %copy-start = (bf16[2048,256]{1,0:T(8,128)(2,1)S(1)}, bf16[2048,256]{1,0:T(8,128)(2,1)}, u32[]{:S(2)}) copy-start(bf16[2048,256]{1,0:T(8,128)(2,1)} %param.21) | copy-start | bytes 3145732
  8.9 23.9 %copy-start.7 = (bf16[128,128]{1,0:T(8,128)(2,1)S(1)}, bf16[128,128]{1,0:T(8,128)(2,1)}, u32[]{:S(2)}) copy-start(bf16[128,128]{1,0:T(8,128)(2,1)} %param.23) | copy-start | bytes 98308
  8.9 23.9 %copy-start.13 = (bf16[128,128]{1,0:T(8,128)(2,1)S(1)}, bf16[128,128]{1,0:T(8,128)(2,1)}, u32[]{:S(2)}) copy-start(bf16[128,128]{1,0:T(8,128)(2,1)} %param.22) | copy-start | bytes 98308
  8.9 24.9 %copy-start.2 = (bf16[32,2048]{1,0:T(8,128)(2,1)S(1)}, bf16[32,2048]{1,0:T(8,128)(2,1)}, u32[]{:S(2)}) copy-start(bf16[32,2048]{1,0:T(8,128)(2,1)} %param.16) | copy-start | bytes 393220
  10.0 24.6 %copy-start.10 = (f32[2048]{0:T(1024)S(1)}, f32[2048]{0:T(1024)}, u32[]{:S(2)}) copy-start(f32[2048]{0:T(1024)} %param.18) | copy-start | bytes 24580
  11.4 0.6 copy-start.5
  12.0 22.9 %copy-start.1 = (bf16[2048,256]{1,0:T(8,128)(2,1)S(1)}, bf16[2048,256]{1,0:T(8,128)(2,1)}, u32[]{:S(2)}) copy-start(bf16[2048,256]{1,0:T(8,128)(2,1)} %param.20) | copy-start | bytes 3145732
  13.8 190.4 %all-to-all-start = ((bf16[64,128,128]{2,1,0:T(8,128)(2,1)}), bf16[64,128,128]{2,1,0:T(8,128)(2,1)}, u32[]{:S(2)}, u32[]{:S(2)}) async-start(bf16[64,128,128]{2,1,0:T(8,128)(2,1)} %stack.11), calls=%async_computation | async-start | bytes 4194304 | tf_op jit(solution)/shard_map/all_to_all | solution.py:161
  32.8 165.6 %all-gather.5.cloned.1.call-start = ((), (), s32[]{:S(2)}) async-start(), calls=%async_computation.6 | async-start | bytes 4259840 | tf_op jit(solution)/shard_map/all_gather | solution.py:17
  32.9 0.9 copy-start.16
  33.8 365.7 %all-gather.3.cloned.1.call-start = ((), (), s32[]{:S(2)}) async-start(), calls=%async_computation.5 | async-start | bytes 8519680 | tf_op jit(solution)/shard_map/all_gather | solution.py:17
  34.0 0.6 copy-start.18
  34.6 13.9 %copy-start.14 = (f32[32]{0:T(128)}, f32[32]{0:T(128)S(1)}, u32[]{:S(2)}) copy-start(f32[32]{0:T(128)S(1)} %fusion.122) | copy-start | bytes 388
  224.8 32.4 %copy-start.12 = (f32[16,512,1]{1,2,0:T(1,128)}, f32[16,512,1]{1,2,0:T(1,128)S(1)}, u32[]{:S(2)}) copy-start(f32[16,512,1]{1,2,0:T(1,128)S(1)} %get-tuple-element.121) | copy-start | bytes 98308
  399.4 5.8 copy-start.4
  399.4 5.8 copy-start.6
  399.4 5.8 copy-start.8
  399.5 5.8 copy-start.17
  405.3 102.7 %copy-start.11 = (f32[2048]{0:T(1024)S(1)}, f32[2048]{0:T(1024)}, u32[]{:S(2)}) copy-start(f32[2048]{0:T(1024)} %param.17) | copy-start | bytes 24580
  488.8 14.6 %all-to-all-start.1 = ((bf16[8,16,2048]{2,1,0:T(8,128)(2,1)}), bf16[8,16,2048]{2,1,0:T(8,128)(2,1)}, u32[]{:S(2)}, u32[]{:S(2)}) async-start(bf16[8,16,2048]{2,1,0:T(8,128)(2,1)} %bitcast.217), calls=%async_computation.1 | async-start | bytes 1048576 | tf_op jit(solution)/shard_map/all_to_all | solution.py:44
  503.4 9.4 %all-to-all-start.3 = ((bf16[8,32,256]{2,1,0:T(8,128)(2,1)}), bf16[8,32,256]{2,1,0:T(8,128)(2,1)S(1)}, u32[]{:S(2)}, u32[]{:S(2)}) async-start(bf16[8,32,256]{2,1,0:T(8,128)(2,1)} %convert_element_type.121), calls=%async_computation.3 | async-start | bytes 262144 | tf_op jit(solution)/shard_map/all_to_all | solution.py:237
  506.8 34.0 %copy-start.3 = (bf16[32,2048]{1,0:T(8,128)(2,1)S(1)}, bf16[32,2048]{1,0:T(8,128)(2,1)}, u32[]{:S(2)}) copy-start(bf16[32,2048]{1,0:T(8,128)(2,1)} %param.16) | copy-start | bytes 393220
  512.8 15.5 %copy-start.9 = (bf16[8,32,256]{2,1,0:T(8,128)(2,1)}, bf16[8,32,256]{2,1,0:T(8,128)(2,1)S(1)}, u32[]{:S(2)}) copy-start(bf16[8,32,256]{2,1,0:T(8,128)(2,1)S(1)} %all-to-all-done.3) | copy-start | bytes 393220
  513.6 27.7 %copy-start.19 = (f32[32]{0:T(128)S(1)}, f32[32]{0:T(128)}, u32[]{:S(2)}) copy-start(f32[32]{0:T(128)} %copy-done.18) | copy-start | bytes 388
  513.6 27.7 %copy-start.15 = (f32[32]{0:T(128)S(1)}, f32[32]{0:T(128)}, u32[]{:S(2)}) copy-start(f32[32]{0:T(128)} %copy-done.14) | copy-start | bytes 388
  513.6 14.6 %all-to-all-start.2 = ((bf16[8,16,2048]{2,1,0:T(8,128)(2,1)}), bf16[8,16,2048]{2,1,0:T(8,128)(2,1)}, u32[]{:S(2)}, u32[]{:S(2)}) async-start(bf16[8,16,2048]{2,1,0:T(8,128)(2,1)} %broadcast_in_dim.22), calls=%async_computation.2 | async-start | bytes 1048576 | tf_op jit(solution)/shard_map/all_to_all | solution.py:56
  528.3 65.9 %all-to-all-start.4 = ((f32[64,32,128]{2,1,0:T(8,128)}), f32[64,32,128]{2,1,0:T(8,128)S(1)}, u32[]{:S(2)}, u32[]{:S(2)}) async-start(f32[64,32,128]{2,1,0:T(8,128)} %fusion.92), calls=%async_computation.4 | async-start | bytes 2097152 | tf_op jit(solution)/shard_map/all_to_all | solution.py:38
Sparse Core Ops, SparseCore 0:
  36.5 161.7 all-gather.4
  201.8 152.1 all-gather.2
